TPU v7x, 256 devices: a whole 4x4x8 slice. The times are simulated.
256 devices in a mesh: sp: 32 (over z, x), tp: 8 (over y, core).
Axes of the slice: x: 4, y: 4, z: 8, core: 2. Of those that a mesh axis runs over, the one named last changes fastest.
Arguments:
- tokens: bfloat16 [16384, 2048], P(('sp', 'tp')), may hold values from -6 to 6
- input_gain: bfloat16 [2048], replicated, may hold values from 0.099609375 to 1.8984375
- weight_query: bfloat16 [2048, 1024], P(None, 'tp'), may hold values from -0.125 to 0.125
- weight_key: bfloat16 [2048, 1024], P(None, 'tp'), may hold values from -0.125 to 0.125
- weight_value: bfloat16 [2048, 2048], P(None, 'tp'), may hold values from -8 to 8
- weight_outgate: bfloat16 [2048, 2048], P(None, 'tp'), may hold values from -0.125 to 0.125
- weight_ingate: bfloat16 [2048, 8], replicated, may hold values from -0.125 to 0.125
- weight_forget: bfloat16 [2048, 8], replicated, may hold values from -0.125 to 0.125
- forget_shift: float32 [16384, 8], P('sp', 'tp'), may hold values from 0 to 20
- mem_gain: bfloat16 [2048], replicated, may hold values from 0.099609375 to 1.8984375
- query_down_weight: bfloat16 [2048, 768], P(None, 'tp'), may hold values from -0.125 to 0.125
- latent_down_weight: bfloat16 [2048, 512], P(None, 'tp'), may hold values from -0.125 to 0.125
- down_rotary: bfloat16 [2048, 64], replicated, may hold values from -0.125 to 0.125
- query_gain: float32 [768], replicated, may hold values from 0.15 to 12
- latent_gain: float32 [512], replicated, may hold values from 0.15 to 12
- query_up_weight: bfloat16 [768, 1536], P(None, 'tp'), may hold values from -0.4375 to 0.4375
- key_up_weight: bfloat16 [512, 1024], P(None, 'tp'), may hold values from -0.25 to 0.25
- value_up_weight: bfloat16 [512, 1024], P(None, 'tp'), may hold values from -0.25 to 0.25
- out_memory: bfloat16 [2048, 2048], P('tp'), may hold values from -0.5 to 0.5
- out_attend: bfloat16 [1024, 2048], P('tp'), may hold values from -0.75 to 0.75
Outputs:
- mixed: bfloat16 [16384, 2048], P(('sp', 'tp'))
All inputs are finite; a program needn't handle non-finite values.
Results may differ from a plain program's by a relative error of at most 0.04.
The roundings to bfloat16 on the way count: a program that leaves them out, or rounds other values in their place, can miss the bound.
Values may be sent and summed in bfloat16 or wider, within the bound.
No kernel may reach another device: no remote copies, remote signals or barrier semaphores. Data moves between devices by JAX's collectives and lax.ppermute only.
A program may use at most 128 MiB of HBM per device.

v0:
```python
import math
import jax
import jax.numpy as jnp
from jax import lax
from jax.sharding import Mesh
from jax.sharding import PartitionSpec as P

MEMORY_HEADS = 8
M_QK = 128
M_V = 256
PLAIN_CHANNELS = 128
ROTARY_CHANNELS = 64
VALUE_CHANNELS = 128
BLOCK = 64
SP = ("sp_0", "sp_1")
SP_TP = ("sp_0", "sp_1", "tp")
SMALL_CONSTANT = 1e-06
SOFTCAP = 15.0
ROTARY_BASE = 10000.0
PRECISE = lax.Precision.HIGHEST
FAR_BELOW = -1e30


def copy_for_each(shard, axis):
    copies = jnp.broadcast_to(shard, (lax.axis_size(axis), *shard.shape))
    return lax.all_to_all(copies, axis, split_axis=0, concat_axis=0, tiled=True)


def laid_out(tiles, dim):
    shape = list(tiles.shape[1:])
    shape[dim] *= tiles.shape[0]
    return jnp.moveaxis(tiles, 0, dim).reshape(shape)


def gather_directly(shard, axis, dim):
    tiles = copy_for_each(shard, axis)
    return laid_out(tiles, dim)


def nothing_yet(shard, identity):
    return jax.tree.map(
        lambda a, e: jnp.broadcast_to(jnp.asarray(e, a.dtype), a.shape), shard, identity
    )


def gathered_once(shard, axis):
    leaves = jax.tree.leaves(shard)
    order = sorted(range(len(leaves)), key=lambda k: -leaves[k].size)
    width = (1, *leaves[order[0]].shape)[-1]
    lines = [
        jnp.pad(leaves[k].reshape(-1), (0, -leaves[k].size % width)).reshape(-1, width)
        for k in order
    ]
    both, at, found = (lax.all_gather(jnp.concatenate(lines), axis), 0, {})
    for k, line in zip(order, lines):
        slab = both[:, at : at + len(line)].reshape(len(both), -1)
        found[k] = slab[:, : leaves[k].size].reshape(-1, *leaves[k].shape)
        at += len(line)
    numbers = iter(range(len(leaves)))
    return jax.tree.map(lambda _: found[next(numbers)], shard)


def entering(shard, axes, combine, identity):
    before = start = nothing_yet(shard, identity)
    running = shard
    for axis in reversed(axes):
        peers, index = (lax.axis_size(axis), lax.axis_index(axis))
        pieces = gathered_once(running, axis)
        inside, running = (start, start)
        for k in range(peers):
            passed = k < index
            running = combine(running, jax.tree.map(lambda part: part[k], pieces))
            inside = jax.tree.map(lambda new, old: jnp.where(passed, new, old), running, inside)
        before = combine(inside, before)
    return before


def side_by_side(arrays, axis, dim, along):
    ends, at = ([], 0)
    for a in arrays[:-1]:
        at += a.shape[along]
        ends.append(at)
    both = jnp.concatenate(arrays, axis=along)
    return tuple(jnp.split(lax.all_gather(both, axis, axis=dim, tiled=True), ends, axis=along))


def in_blocks(shard, dim, peers):
    shape = shard.shape
    tiles = shard.reshape(*shape[:dim], peers, shape[dim] // peers, *shape[dim + 1 :])
    return jnp.moveaxis(tiles, dim, 0)


def sum_at_owner(shard, axis, dim):
    tiles = in_blocks(shard, dim, lax.axis_size(axis))
    arrived = lax.all_to_all(tiles, axis, split_axis=0, concat_axis=0, tiled=True)
    return arrived.astype(jnp.float32).sum(axis=0)


def rms_scale(values, gain):
    widened = values.astype(jnp.float32)
    return (
        widened
        * lax.rsqrt(jnp.mean(widened * widened, axis=-1, keepdims=True) + SMALL_CONSTANT)
        * gain.astype(jnp.float32)
    )


def rotate(values, positions):
    halfway = values.shape[-1] // 2
    inverse = jnp.power(ROTARY_BASE, -jnp.arange(halfway, dtype=jnp.float32) / halfway)
    angles = positions.astype(jnp.float32)[:, None] * inverse
    cosine = jnp.cos(angles)
    sine_part = jnp.sin(angles)
    if values.ndim == 3:
        cosine = cosine[:, None, :]
        sine_part = sine_part[:, None, :]
    widened = values.astype(jnp.float32)
    first = widened[..., :halfway]
    second = widened[..., halfway:]
    turned = jnp.concatenate(
        [first * cosine - second * sine_part, second * cosine + first * sine_part], axis=-1
    )
    return turned.astype(jnp.bfloat16)


def update_state(carried, key_rows, value_rows, input_gate, cumulative):
    matrix, normal, stabilizer = carried
    last_total = cumulative[:, -1]
    weight_log = last_total[:, None] - cumulative + input_gate
    new_max = jnp.maximum(last_total + stabilizer, jnp.max(weight_log, axis=-1))
    weights = jnp.exp(weight_log - new_max[:, None])
    decay = jnp.exp(last_total + stabilizer - new_max)
    matrix = decay[:, None, None] * matrix + jnp.einsum(
        "hsv,hsd->hvd", weights[:, :, None] * value_rows, key_rows, precision=PRECISE
    )
    normal = decay[:, None] * normal + jnp.einsum(
        "hs,hsd->hd", weights, key_rows, precision=PRECISE
    )
    return (matrix, normal, new_max)


def block_step(carried, inputs):
    query_rows, key_rows, value_rows, input_gate, log_forget = inputs
    matrix, normal, stabilizer = carried
    cumulative = jnp.cumsum(log_forget, axis=-1)
    block_len = log_forget.shape[-1]
    causal = jnp.tril(jnp.ones((block_len, block_len), dtype=bool))
    pair_log = cumulative[:, :, None] - cumulative[:, None, :] + input_gate[:, None, :]
    pair_log = jnp.where(causal, pair_log, -jnp.inf)
    carried_log = cumulative + stabilizer[:, None]
    row_max = jnp.maximum(carried_log, jnp.max(pair_log, axis=-1))
    within = jnp.exp(pair_log - row_max[:, :, None])
    across = jnp.exp(carried_log - row_max)
    affinity = jnp.einsum("hjd,hsd->hjs", query_rows, key_rows, precision=PRECISE) * within
    numerator = jnp.einsum("hjs,hsv->hjv", affinity, value_rows, precision=PRECISE)
    numerator = numerator + across[:, :, None] * jnp.einsum(
        "hjd,hvd->hjv", query_rows, matrix, precision=PRECISE
    )
    denominator = jnp.sum(affinity, axis=-1) + across * jnp.einsum(
        "hjd,hd->hj", query_rows, normal, precision=PRECISE
    )
    output = numerator / jnp.maximum(jnp.abs(denominator), jnp.exp(-row_max))[:, :, None]
    return (update_state(carried, key_rows, value_rows, input_gate, cumulative), output)


def summary_step(carried, inputs):
    key_rows, value_rows, input_gate, log_forget = inputs
    return (
        update_state(carried, key_rows, value_rows, input_gate, jnp.cumsum(log_forget, axis=-1)),
        None,
    )


def merge_states(earlier, later):
    decayed = later[3] + earlier[2]
    joined = jnp.maximum(decayed, later[2])
    early_part = jnp.exp(decayed - joined)
    late_part = jnp.exp(later[2] - joined)
    return (
        early_part[:, None, None] * earlier[0] + late_part[:, None, None] * later[0],
        early_part[:, None] * earlier[1] + late_part[:, None] * later[1],
        joined,
        earlier[3] + later[3],
    )


def per_device(
    tokens,
    input_gain,
    weight_query,
    weight_key,
    weight_value,
    weight_outgate,
    weight_ingate,
    weight_forget,
    forget_shift,
    mem_gain,
    query_down_weight,
    latent_down_weight,
    down_rotary,
    query_gain,
    latent_gain,
    query_up_weight,
    key_up_weight,
    value_up_weight,
    out_memory,
    out_attend,
):
    normed = rms_scale(tokens, input_gain).astype(jnp.bfloat16)
    tp_index = lax.axis_index("tp")
    mem_heads = weight_query.shape[1] // M_QK
    att_heads = key_up_weight.shape[1] // PLAIN_CHANNELS
    ingate_cols = lax.dynamic_slice_in_dim(weight_ingate, tp_index * mem_heads, mem_heads, 1)
    forget_cols = lax.dynamic_slice_in_dim(weight_forget, tp_index * mem_heads, mem_heads, 1)
    weight_list = (
        weight_query,
        weight_key,
        weight_value,
        weight_outgate,
        query_down_weight,
        latent_down_weight,
        down_rotary,
        ingate_cols,
        forget_cols,
    )

    def project(portion):
        return jnp.concatenate(
            [
                jnp.dot(portion, weight, preferred_element_type=jnp.float32)
                for weight in weight_list
            ],
            axis=1,
        )

    projected = project(gather_directly(normed, "tp", 0))
    sections = []
    offset = 0
    for weight in weight_list:
        sections.append(projected[:, offset : offset + weight.shape[1]])
        offset = offset + weight.shape[1]
    stored = tuple((section.astype(jnp.bfloat16) for section in sections[:7]))
    mem_query, mem_key, mem_value, mem_outgate, query_latent, keyval_latent, key_raw = (
        lax.optimization_barrier(stored)
    )
    in_gate = SOFTCAP * jnp.tanh(sections[7] / SOFTCAP)
    log_forget = jax.nn.log_sigmoid(SOFTCAP * jnp.tanh((sections[8] + forget_shift) / SOFTCAP))
    length = projected.shape[0]
    positions = lax.axis_index(SP) * length + jnp.arange(length, dtype=jnp.int32)
    query_whole, latent_whole = (
        lax.all_gather(query_latent, "tp", axis=1, tiled=True),
        lax.all_gather(keyval_latent, "tp", axis=1, tiled=True),
    )
    normed_query = rms_scale(query_whole, query_gain).astype(jnp.bfloat16)
    normed_latent = rms_scale(latent_whole, latent_gain).astype(jnp.bfloat16)
    block_count = length // BLOCK

    def to_blocks(array, width):
        return (
            array.astype(jnp.float32)
            .reshape(block_count, BLOCK, mem_heads, width)
            .transpose(0, 2, 1, 3)
        )

    def gate_blocks(array):
        return array.reshape(block_count, BLOCK, mem_heads).transpose(0, 2, 1)

    query_blocks = to_blocks(mem_query, M_QK)
    key_blocks = to_blocks(mem_key, M_QK) * M_QK ** (-0.5)
    value_blocks = to_blocks(mem_value, M_V)
    ingate_blocks = gate_blocks(in_gate)
    forget_blocks = gate_blocks(log_forget)
    empty_state = (
        jnp.zeros((mem_heads, M_V, M_QK), jnp.float32),
        jnp.zeros((mem_heads, M_QK), jnp.float32),
        jnp.full((mem_heads,), FAR_BELOW, jnp.float32),
    )
    local_state, _ = lax.scan(
        summary_step, empty_state, (key_blocks, value_blocks, ingate_blocks, forget_blocks)
    )
    identity = empty_state + (jnp.zeros((mem_heads,), jnp.float32),)
    prefix = entering(
        (local_state[0], local_state[1], local_state[2], jnp.sum(log_forget, axis=0)),
        SP,
        merge_states,
        identity,
    )
    start_max = jnp.maximum(prefix[3], prefix[2])
    rescale = jnp.exp(prefix[2] - start_max)
    initial = (prefix[0] * rescale[:, None, None], prefix[1] * rescale[:, None], start_max)
    _, cell = lax.scan(
        block_step, initial, (query_blocks, key_blocks, value_blocks, ingate_blocks, forget_blocks)
    )
    cell = cell.transpose(0, 2, 1, 3).reshape(length, mem_heads * M_V)
    cell_total = lax.psum(jnp.sum(cell * cell, axis=1), "tp")
    gain_part = lax.dynamic_slice_in_dim(mem_gain, tp_index * mem_heads * M_V, mem_heads * M_V, 0)
    gated = (
        cell
        * lax.rsqrt(cell_total / (MEMORY_HEADS * M_V) + SMALL_CONSTANT)[:, None]
        * gain_part.astype(jnp.float32)
    )
    gated = gated * jax.nn.sigmoid(mem_outgate.astype(jnp.float32))
    gated = gated.astype(jnp.bfloat16)
    query_all = jnp.dot(normed_query, query_up_weight, preferred_element_type=jnp.float32).astype(
        jnp.bfloat16
    )
    query_all = query_all.reshape(length, att_heads, PLAIN_CHANNELS + ROTARY_CHANNELS)
    query_nope = query_all[..., :PLAIN_CHANNELS]
    query_rot = rotate(query_all[..., PLAIN_CHANNELS:], positions)
    key_rot = rotate(key_raw, positions)
    factor = (PLAIN_CHANNELS + ROTARY_CHANNELS) ** (-0.5)

    def attend_block(carried, key_nope, key_rotary, value_rows, key_start):
        row_max, summed, accum = carried
        number = key_nope.shape[0]
        key_pos = key_start + jnp.arange(number, dtype=jnp.int32)
        scores = jnp.einsum(
            "qhd,khd->hqk",
            query_nope,
            key_nope.reshape(number, att_heads, PLAIN_CHANNELS),
            preferred_element_type=jnp.float32,
        )
        scores = (
            scores
            + jnp.einsum("qhd,kd->hqk", query_rot, key_rotary, preferred_element_type=jnp.float32)
        ) * factor
        allowed = key_pos[None, :] <= positions[:, None]
        scores = jnp.where(allowed[None], scores, -jnp.inf)
        new_max = jnp.maximum(row_max, jnp.max(scores, axis=-1))
        probs = jnp.exp(scores - new_max[:, :, None])
        shrink = jnp.exp(row_max - new_max)
        summed = summed * shrink + jnp.sum(probs, axis=-1)
        accum = accum * shrink[:, :, None] + jnp.einsum(
            "hqk,khd->hqd",
            probs.astype(jnp.bfloat16),
            value_rows.reshape(number, att_heads, VALUE_CHANNELS),
            preferred_element_type=jnp.float32,
        )
        return (new_max, summed, accum)

    initial_att = (
        jnp.full((att_heads, length), FAR_BELOW, jnp.float32),
        jnp.zeros((att_heads, length), jnp.float32),
        jnp.zeros((att_heads, length, VALUE_CHANNELS), jnp.float32),
    )
    own_nope = jnp.dot(normed_latent, key_up_weight, preferred_element_type=jnp.float32).astype(
        jnp.bfloat16
    )
    own_values = jnp.dot(normed_latent, value_up_weight, preferred_element_type=jnp.float32).astype(
        jnp.bfloat16
    )
    carried = initial_att
    piece_rows = side_by_side((own_nope, key_rot, own_values), SP, 0, 1)
    number = piece_rows[0].shape[0]
    size = math.gcd(number, 1024)

    def one_block(state, block_number):
        begin = block_number * size
        sub_rows = tuple(
            (lax.dynamic_slice_in_dim(member, begin, size, 0) for member in piece_rows)
        )

        def compute(current):
            key_nope, key_rotary, value_rows = sub_rows
            return attend_block(current, key_nope, key_rotary, value_rows, begin)

        return (
            lax.cond(begin <= positions[length - 1], compute, lambda current: current, state),
            None,
        )

    carried, _ = lax.scan(one_block, carried, jnp.arange(number // size, dtype=jnp.int32))
    attended = (carried[2] / carried[1][:, :, None]).astype(jnp.bfloat16)
    attended = attended.transpose(1, 0, 2).reshape(length, att_heads * VALUE_CHANNELS)
    mixed = sum_at_owner(
        (
            jnp.dot(gated, out_memory, preferred_element_type=jnp.float32)
            + jnp.dot(attended, out_attend, preferred_element_type=jnp.float32)
        ).astype(jnp.bfloat16),
        "tp",
        0,
    )
    return mixed.astype(jnp.bfloat16)


def solution(mesh):
    torus = Mesh(mesh.devices.reshape(8, 4, mesh.shape["tp"]), ("sp_0", "sp_1", "tp"))
    in_specs = (
        P(SP_TP, None),
        P(),
        P(None, "tp"),
        P(None, "tp"),
        P(None, "tp"),
        P(None, "tp"),
        P(),
        P(),
        P(SP, "tp"),
        P(),
        P(None, "tp"),
        P(None, "tp"),
        P(),
        P(),
        P(),
        P(None, "tp"),
        P(None, "tp"),
        P(None, "tp"),
        P("tp", None),
        P("tp", None),
    )
    out_specs = P(SP_TP, None)
    return jax.shard_map(
        per_device, mesh=torus, in_specs=in_specs, out_specs=out_specs, check_vma=False
    )
```

profile of v0, /device:TPU:230, one launch (start us, length us, event | category | flops | bytes accessed | tf_op | source)
XLA Modules:
  0.0 451.5 jit_solution(11439639850587882562)
XLA Ops:
  15.7 27.1 %all-to-all-done = bf16[8,64,2048]{2,1,0:T(8,128)(2,1)S(1)} async-done(((bf16[8,64,2048]{2,1,0:T(8,128)(2,1)}), bf16[8,64,2048]{2,1,0:T(8,128)(2,1)S(1)}, u32[]{:S(2)}, u32[]{:S(2)}) %all-to-all-start) | async-done | bytes 2097184 | tf_op jit(solution)/shard_map/all_to_all | solution.py:26
  54.4 40.7 %while.47 = (s32[]{:T(128)}, f32[1,256,128]{2,1,0:T(8,128)S(1)}, f32[1,128]{1,0:T(1,128)S(1)}, f32[1]{0:T(128)}, f32[8,1,64]{2,1,0:T(1,128)S(1)}, /*index=5*/f32...) while((s32[]{:T(128)}, f32[1,256,128]{2,1,0:T(8,128)S(1)}, ...), condition=%wide.region_4.5_spmd.clone, body=%wide.region_1.0_spmd.clone.sunk | while | flops 25383812 | bytes 401378 | solution.py:278
  95.1 13.5 %all-gather.2 = f32[4,259,128]{2,1,0:T(8,128)S(1)} all-gather(f32[1,259,128]{2,1,0:T(8,128)S(1)} %maximum_bitcast_fusion), channel_id=2, replica_groups=mesh['sp_0'=8,'sp_1'=4,'tp'=8] {'sp_1'}, dimensions={0}, use_global_device_ids=true | all-gather | bytes 663040 | tf_op jit(solution)/shard_map/all_gather | solution.py:54
  120.6 13.1 %all_gather.25 = bf16[512,512]{0,1:T(8,128)(2,1)S(1)} all-gather(bf16[512,64]{0,1:T(8,128)(2,1)S(1)} %copy-done.8), channel_id=1, replica_groups=mesh['sp_0'=8,'sp_1'=4,'tp'=8] {'tp'}, dimensions={1}, use_global_device_ids=true | all-gather | bytes 589824 | tf_op jit(solution)/shard_map/all_gather | solution.py:252
  138.0 13.4 %all_gather.27 = bf16[512,768]{0,1:T(8,128)(2,1)S(1)} all-gather(bf16[512,96]{0,1:T(8,128)(2,1)S(1)} %convolution_convert_fusion.7), channel_id=1, replica_groups=mesh['sp_0'=8,'sp_1'=4,'tp'=8] {'tp'}, dimensions={1}, use_global_device_ids=true | all-gather | bytes 884736 | tf_op jit(solution)/shard_map/all_gather | solution.py:251
  180.6 68.9 %while.45 = (s32[]{:T(128)}, f32[1,256,128]{2,1,0:T(8,128)S(1)}, f32[1,128]{1,0:T(1,128)S(1)}, f32[1]{0:T(128)}, f32[8,1,64,256]{3,2,1,0:T(8,128)S(1)}, /*index=...) while((s32[]{:T(128)}, f32[1,256,128]{2,1,0:T(8,128)S(1)}, ...), condition=%wide.region_11.12_spmd, body=%wide.region_6.11_spmd.sunk | while | flops 69588096 | bytes 982777 | solution.py:291
  249.7 13.4 %psum.7 = f32[512]{0:T(512)S(1)} all-reduce(f32[512]{0:T(512)S(1)} %reduce_sum.82), channel_id=1, replica_groups=mesh['sp_0'=8,'sp_1'=4,'tp'=8] {'tp'}, use_global_device_ids=true, to_apply=%region_13.14 | all-reduce | flops 512 | bytes 4096 | tf_op jit(solution)/shard_map/psum | solution.py:295
  269.7 6.0 %fusion.169 = (bf16[16384,128]{0,1:T(8,128)(2,1)}, bf16[16384,128]{0,1:T(8,128)(2,1)}) fusion(bf16[16384,320]{0,1:T(8,128)(2,1)} %all-gather.7.cloned.1.call-done), kind=kLoop, calls=%fused_computation.273 | loop fusion | bytes 16777216 | tf_op jit(solution)/shard_map/split | solution.py:84
  275.7 6.4 %copy.48 = bf16[16384,128]{1,0:T(8,128)(2,1)} copy(bf16[16384,128]{0,1:T(8,128)(2,1)} %get-tuple-element.494) | data formatting | bytes 8388608 | tf_op jit(solution)/shard_map/while | solution.py:372
  286.8 6.4 %copy.45 = bf16[16384,128]{1,0:T(8,128)(2,1)} copy(bf16[16384,128]{0,1:T(8,128)(2,1)} %get-tuple-element.495) | data formatting | bytes 8388608 | tf_op jit(solution)/shard_map/while | solution.py:372
  293.2 116.5 %while.46 = (s32[]{:T(128)}, f32[1,512]{1,0:T(1,128)S(1)}, f32[1,512]{1,0:T(1,128)S(1)}, f32[1,512,128]{2,1,0:T(8,128)S(1)}, s32[16]{0:T(128)S(1)}, /*index=5*/s...) while((s32[]{:T(128)}, f32[1,512]{1,0:T(1,128)S(1)}, ...), condition=%wide.region_21.22_spmd, body=%wide.region_16.21_spmd.sunk | while | flops 340396032 | bytes 12036461 | solution.py:372
  295.7 4.9 %conditional.2 = ((f32[1,512]{1,0:T(1,128)S(1)}, f32[1,512]{1,0:T(1,128)S(1)}, f32[1,512,128]{2,1,0:T(8,128)S(1)})) conditional(s32[]{:T(128)} %convert_element_type.198, (f32[1,512]{1,0:T(1,128)S(1)}, f32[1,512]{1,0:T(1,128)S(1)}, f32[1,512,128]{2,1,0:T(8,128)S(1)}) %tuple.113, (s32[]{:T(128)}, s32[512]{0:T(512)S(1)}, ...), branch_computations={%region_17.17_spmd, %region_18.20_spmd} | conditional | flops 340396032 | bytes 12036178 | solution.py:368
  310.2 4.9 %conditional.2 = ((f32[1,512]{1,0:T(1,128)S(1)}, f32[1,512]{1,0:T(1,128)S(1)}, f32[1,512,128]{2,1,0:T(8,128)S(1)})) conditional(s32[]{:T(128)} %convert_element_type.198, (f32[1,512]{1,0:T(1,128)S(1)}, f32[1,512]{1,0:T(1,128)S(1)}, f32[1,512,128]{2,1,0:T(8,128)S(1)}) %tuple.113, (s32[]{:T(128)}, s32[512]{0:T(512)S(1)}, ...), branch_computations={%region_17.17_spmd, %region_18.20_spmd} | conditional | flops 340396032 | bytes 12036178 | solution.py:368
  317.5 4.9 %conditional.2 = ((f32[1,512]{1,0:T(1,128)S(1)}, f32[1,512]{1,0:T(1,128)S(1)}, f32[1,512,128]{2,1,0:T(8,128)S(1)})) conditional(s32[]{:T(128)} %convert_element_type.198, (f32[1,512]{1,0:T(1,128)S(1)}, f32[1,512]{1,0:T(1,128)S(1)}, f32[1,512,128]{2,1,0:T(8,128)S(1)}) %tuple.113, (s32[]{:T(128)}, s32[512]{0:T(512)S(1)}, ...), branch_computations={%region_17.17_spmd, %region_18.20_spmd} | conditional | flops 340396032 | bytes 12036178 | solution.py:368
  324.8 4.9 %conditional.2 = ((f32[1,512]{1,0:T(1,128)S(1)}, f32[1,512]{1,0:T(1,128)S(1)}, f32[1,512,128]{2,1,0:T(8,128)S(1)})) conditional(s32[]{:T(128)} %convert_element_type.198, (f32[1,512]{1,0:T(1,128)S(1)}, f32[1,512]{1,0:T(1,128)S(1)}, f32[1,512,128]{2,1,0:T(8,128)S(1)}) %tuple.113, (s32[]{:T(128)}, s32[512]{0:T(512)S(1)}, ...), branch_computations={%region_17.17_spmd, %region_18.20_spmd} | conditional | flops 340396032 | bytes 12036178 | solution.py:368
  332.1 4.9 %conditional.2 = ((f32[1,512]{1,0:T(1,128)S(1)}, f32[1,512]{1,0:T(1,128)S(1)}, f32[1,512,128]{2,1,0:T(8,128)S(1)})) conditional(s32[]{:T(128)} %convert_element_type.198, (f32[1,512]{1,0:T(1,128)S(1)}, f32[1,512]{1,0:T(1,128)S(1)}, f32[1,512,128]{2,1,0:T(8,128)S(1)}) %tuple.113, (s32[]{:T(128)}, s32[512]{0:T(512)S(1)}, ...), branch_computations={%region_17.17_spmd, %region_18.20_spmd} | conditional | flops 340396032 | bytes 12036178 | solution.py:368
  339.4 4.9 %conditional.2 = ((f32[1,512]{1,0:T(1,128)S(1)}, f32[1,512]{1,0:T(1,128)S(1)}, f32[1,512,128]{2,1,0:T(8,128)S(1)})) conditional(s32[]{:T(128)} %convert_element_type.198, (f32[1,512]{1,0:T(1,128)S(1)}, f32[1,512]{1,0:T(1,128)S(1)}, f32[1,512,128]{2,1,0:T(8,128)S(1)}) %tuple.113, (s32[]{:T(128)}, s32[512]{0:T(512)S(1)}, ...), branch_computations={%region_17.17_spmd, %region_18.20_spmd} | conditional | flops 340396032 | bytes 12036178 | solution.py:368
  346.7 4.9 %conditional.2 = ((f32[1,512]{1,0:T(1,128)S(1)}, f32[1,512]{1,0:T(1,128)S(1)}, f32[1,512,128]{2,1,0:T(8,128)S(1)})) conditional(s32[]{:T(128)} %convert_element_type.198, (f32[1,512]{1,0:T(1,128)S(1)}, f32[1,512]{1,0:T(1,128)S(1)}, f32[1,512,128]{2,1,0:T(8,128)S(1)}) %tuple.113, (s32[]{:T(128)}, s32[512]{0:T(512)S(1)}, ...), branch_computations={%region_17.17_spmd, %region_18.20_spmd} | conditional | flops 340396032 | bytes 12036178 | solution.py:368
  353.9 4.9 %conditional.2 = ((f32[1,512]{1,0:T(1,128)S(1)}, f32[1,512]{1,0:T(1,128)S(1)}, f32[1,512,128]{2,1,0:T(8,128)S(1)})) conditional(s32[]{:T(128)} %convert_element_type.198, (f32[1,512]{1,0:T(1,128)S(1)}, f32[1,512]{1,0:T(1,128)S(1)}, f32[1,512,128]{2,1,0:T(8,128)S(1)}) %tuple.113, (s32[]{:T(128)}, s32[512]{0:T(512)S(1)}, ...), branch_computations={%region_17.17_spmd, %region_18.20_spmd} | conditional | flops 340396032 | bytes 12036178 | solution.py:368
  361.2 4.9 %conditional.2 = ((f32[1,512]{1,0:T(1,128)S(1)}, f32[1,512]{1,0:T(1,128)S(1)}, f32[1,512,128]{2,1,0:T(8,128)S(1)})) conditional(s32[]{:T(128)} %convert_element_type.198, (f32[1,512]{1,0:T(1,128)S(1)}, f32[1,512]{1,0:T(1,128)S(1)}, f32[1,512,128]{2,1,0:T(8,128)S(1)}) %tuple.113, (s32[]{:T(128)}, s32[512]{0:T(512)S(1)}, ...), branch_computations={%region_17.17_spmd, %region_18.20_spmd} | conditional | flops 340396032 | bytes 12036178 | solution.py:368
  368.5 4.9 %conditional.2 = ((f32[1,512]{1,0:T(1,128)S(1)}, f32[1,512]{1,0:T(1,128)S(1)}, f32[1,512,128]{2,1,0:T(8,128)S(1)})) conditional(s32[]{:T(128)} %convert_element_type.198, (f32[1,512]{1,0:T(1,128)S(1)}, f32[1,512]{1,0:T(1,128)S(1)}, f32[1,512,128]{2,1,0:T(8,128)S(1)}) %tuple.113, (s32[]{:T(128)}, s32[512]{0:T(512)S(1)}, ...), branch_computations={%region_17.17_spmd, %region_18.20_spmd} | conditional | flops 340396032 | bytes 12036178 | solution.py:368
  375.8 4.9 %conditional.2 = ((f32[1,512]{1,0:T(1,128)S(1)}, f32[1,512]{1,0:T(1,128)S(1)}, f32[1,512,128]{2,1,0:T(8,128)S(1)})) conditional(s32[]{:T(128)} %convert_element_type.198, (f32[1,512]{1,0:T(1,128)S(1)}, f32[1,512]{1,0:T(1,128)S(1)}, f32[1,512,128]{2,1,0:T(8,128)S(1)}) %tuple.113, (s32[]{:T(128)}, s32[512]{0:T(512)S(1)}, ...), branch_computations={%region_17.17_spmd, %region_18.20_spmd} | conditional | flops 340396032 | bytes 12036178 | solution.py:368
  390.4 4.9 %conditional.2 = ((f32[1,512]{1,0:T(1,128)S(1)}, f32[1,512]{1,0:T(1,128)S(1)}, f32[1,512,128]{2,1,0:T(8,128)S(1)})) conditional(s32[]{:T(128)} %convert_element_type.198, (f32[1,512]{1,0:T(1,128)S(1)}, f32[1,512]{1,0:T(1,128)S(1)}, f32[1,512,128]{2,1,0:T(8,128)S(1)}) %tuple.113, (s32[]{:T(128)}, s32[512]{0:T(512)S(1)}, ...), branch_computations={%region_17.17_spmd, %region_18.20_spmd} | conditional | flops 340396032 | bytes 12036178 | solution.py:368
  412.8 30.7 %all_to_all.10 = bf16[8,64,2048]{2,1,0:T(8,128)(2,1)S(1)} all-to-all(bf16[8,64,2048]{2,1,0:T(8,128)(2,1)S(1)} %bitcast.447), channel_id=1, replica_groups=mesh['sp_0'=8,'sp_1'=4,'tp'=8] {'tp'}, dimensions={0} | all-to-all | bytes 4194304 | tf_op jit(solution)/shard_map/all_to_all | solution.py:95
  (436 shorter events, 253.5 us)
Async XLA Ops:
  6.5 256.8 %copy-start = (bf16[256,2048]{1,0:T(8,128)(2,1)S(1)}, bf16[256,2048]{1,0:T(8,128)(2,1)}, u32[]{:S(2)}) copy-start(bf16[256,2048]{1,0:T(8,128)(2,1)} %param.46) | copy-start | bytes 3145732
  11.1 31.6 %all-to-all-start = ((bf16[8,64,2048]{2,1,0:T(8,128)(2,1)}), bf16[8,64,2048]{2,1,0:T(8,128)(2,1)S(1)}, u32[]{:S(2)}, u32[]{:S(2)}) async-start(bf16[8,64,2048]{2,1,0:T(8,128)(2,1)} %broadcast_in_dim.36), calls=%async_computation | async-start | bytes 4194304 | tf_op jit(solution)/shard_map/all_to_all | solution.py:26
  15.6 28.7 %copy-start.10 = (f32[512,1]{0,1:T(1,128)S(1)}, f32[512,1]{0,1:T(1,128)}, u32[]{:S(2)}) copy-start(f32[512,1]{0,1:T(1,128)} %param.36) | copy-start | bytes 6148
  15.6 139.8 %all-gather.9.cloned.1.call-start = ((), (), s32[]{:S(2)}) async-start(), calls=%async_computation.3 | async-start | bytes 1216512 | tf_op jit(solution)/shard_map/all_gather | solution.py:54
  42.8 4.3 copy-start.5
  47.1 1.4 copy-start.6
  47.1 2.8 copy-start.4
  48.5 2.2 copy-start.1
  49.9 1.5 copy-start.2
  50.7 1.5 copy-start.11
  52.1 1.4 copy-start.12
  54.4 66.3 %copy-start.9 = (bf16[512,64]{0,1:T(8,128)(2,1)S(1)}, bf16[512,64]{0,1:T(8,128)(2,1)}, u32[]{:S(2)}) copy-start(bf16[512,64]{0,1:T(8,128)(2,1)} %convolution_convert_fusion.8) | copy-start | bytes 196612
  54.4 66.3 %copy-start.8 = (bf16[512,64]{0,1:T(8,128)(2,1)S(1)}, bf16[512,64]{0,1:T(8,128)(2,1)}, u32[]{:S(2)}) copy-start(bf16[512,64]{0,1:T(8,128)(2,1)} %convolution_convert_fusion.9) | copy-start | bytes 196612
  95.0 39.2 %copy-start.13 = (bf16[512,128]{1,0:T(8,128)(2,1)S(1)}, bf16[512,128]{1,0:T(8,128)(2,1)}, u32[]{:S(2)}) copy-start(bf16[512,128]{1,0:T(8,128)(2,1)} %param.45) | copy-start | bytes 393220
  95.1 39.2 %copy-start.16 = (f32[512]{0:T(512)S(1)}, f32[512]{0:T(512)}, u32[]{:S(2)}) copy-start(f32[512]{0:T(512)} %param.42) | copy-start | bytes 6148
  108.6 26.0 %copy-start.14 = (bf16[512,128]{1,0:T(8,128)(2,1)S(1)}, bf16[512,128]{1,0:T(8,128)(2,1)}, u32[]{:S(2)}) copy-start(bf16[512,128]{1,0:T(8,128)(2,1)} %param.44) | copy-start | bytes 393220
  120.5 149.1 %all-gather.7.cloned.1.call-start = ((), (), s32[]{:S(2)}) async-start(), calls=%async_computation.2 | async-start | bytes 10813440 | tf_op jit(solution)/shard_map/all_gather | solution.py:84
  134.6 17.0 %copy-start.15 = (f32[768]{0:T(1024)S(1)}, f32[768]{0:T(1024)}, u32[]{:S(2)}) copy-start(f32[768]{0:T(1024)} %param.41) | copy-start | bytes 9220
  180.6 82.6 %copy-start.7 = (bf16[512,256]{1,0:T(8,128)(2,1)S(1)}, bf16[512,256]{1,0:T(8,128)(2,1)}, u32[]{:S(2)}) copy-start(bf16[512,256]{1,0:T(8,128)(2,1)} %convolution_convert_fusion) | copy-start | bytes 786436
  282.1 1.6 slice-start
  293.2 116.6 %copy-start.3 = (bf16[128,2048]{1,0:T(8,128)(2,1)S(1)}, bf16[128,2048]{1,0:T(8,128)(2,1)}, u32[]{:S(2)}) copy-start(bf16[128,2048]{1,0:T(8,128)(2,1)} %param.47) | copy-start | bytes 1572868
Sparse Core Ops, SparseCore 0:
  120.6 34.7 all-gather.8
  157.9 111.7 all-gather.6
where the time goes:
time: 457 us; the launch traced here: 451 us
  matrix products  134 us (29%)
  blocking collectives  84.2 us (18%)
  local copies, waits for them, and re-layouts  57.2 us (13%)
  other arithmetic  51.3 us (11%)
  between operations  45.9 us (10%)
  loops' own time  41.5 us (9%)
  waiting for transfers between devices  32.6 us (7%)
    all_to_all x1, blocking collectives, sum_at_owner(): lax.all_to_all(tiles, axis, split_axis=0, concat_axis=0, tiled=True)  30.7 us
    all_to_all x1, waiting for transfers between devices, copy_for_each(): return lax.all_to_all(copies, axis, split_axis=0, concat_axis=0, tiled=True)  27.1 us
    dot_general x16, matrix products, attend_block(): jnp.einsum('hqk,khd->hqd', probs.astype(jnp.bfloat16), value_rows.reshape...  24.4 us
    dot_general x16, matrix products, attend_block(): jnp.einsum('qhd,kd->hqk', query_rot, key_rotary, preferred_element_type=j...  23.9 us
    dot_general x16, matrix products, attend_block(): jnp.einsum('qhd,khd->hqk', query_nope, key_nope.reshape(number, att_heads...  22.4 us
    another operation x1, loops' own time, per_device(): lax.scan(one_block, carried, jnp.arange(number // size, dtype=jnp.int32))  20 us
    reduce_max x16, other arithmetic, update_state(): new_max = jnp.maximum(last_total + stabilizer, jnp.max(weight_log, axis=-1))  19.6 us
    while x4, local copies, waits for them, and re-layouts, per_device(): lax.scan(one_block, carried, jnp.arange(number // size, dtype=jnp.int32))  16 us
  transfers between devices with their start and end apart: 3, of which 3 were waited for; matrix products, arithmetic and copies ran while one was open for 16% of the time, Pallas kernels for 0%

commit v1 on v0

--- a/solution.py
+++ b/solution.py
@@ -4,6 +4,7 @@
 from jax import lax
 from jax.sharding import Mesh
 from jax.sharding import PartitionSpec as P
+from jax.lax import all_to_all, axis_size
 
 MEMORY_HEADS = 8
 M_QK = 128
@@ -248,7 +249,10 @@
     length = projected.shape[0]
     positions = lax.axis_index(SP) * length + jnp.arange(length, dtype=jnp.int32)
     query_whole, latent_whole = (
-        lax.all_gather(query_latent, "tp", axis=1, tiled=True),
+        jnp.concatenate(
+            all_to_all(jnp.stack([query_latent for _ in range(axis_size("tp"))]), "tp", 0, 0),
+            axis=1,
+        ),
         lax.all_gather(keyval_latent, "tp", axis=1, tiled=True),
     )
     normed_query = rms_scale(query_whole, query_gain).astype(jnp.bfloat16)

time: 457 us -> 466 us (1.020)
  blocking collectives: 84.2 us -> 70.1 us
  local copies, waits for them, and re-layouts: 57.2 us -> 65.4 us
  waiting for transfers between devices: 32.6 us -> 37.9 us
    all_gather x1 -> x0, blocking collectives: 13.4 us -> none  [per_device(): lax.all_gather(query_latent, 'tp', axis=1, tiled=True)]
    all_to_all x0 -> x1, waiting for transfers between devices: none -> 10.8 us  [per_device(): all_to_all(jnp.stack([query_latent for _ in range(axis_size('tp'))]), 'tp...]
    squeeze x24, local copies, waits for them, and re-layouts: 0.21 us -> 5.2 us  [per_device(): lax.scan(summary_step, empty_state, (key_blocks, value_blocks, ingate_blo...]
  transfers between devices with their start and end apart: 3 -> 4, of which waited for: 3 -> 2; matrix products, arithmetic and copies ran while one was open for 16% -> 17% of each run, Pallas kernels for 0% -> 0%
where the time goes in v1:
time: 466 us; the launch traced here: 460 us
  matrix products  135 us (29%)
  blocking collectives  70.1 us (15%)
  local copies, waits for them, and re-layouts  65.4 us (14%)
  other arithmetic  53.7 us (12%)
  between operations  47.1 us (10%)
  loops' own time  43.1 us (9%)
  waiting for transfers between devices  37.9 us (8%)
  starting transfers between devices  8.1 us (2%)
    all_to_all x1, blocking collectives, sum_at_owner(): lax.all_to_all(tiles, axis, split_axis=0, concat_axis=0, tiled=True)  29.8 us
    all_to_all x1, waiting for transfers between devices, copy_for_each(): return lax.all_to_all(copies, axis, split_axis=0, concat_axis=0, tiled=True)  27.1 us
    dot_general x16, matrix products, attend_block(): jnp.einsum('hqk,khd->hqd', probs.astype(jnp.bfloat16), value_rows.reshape...  24.4 us
    dot_general x16, matrix products, attend_block(): jnp.einsum('qhd,kd->hqk', query_rot, key_rotary, preferred_element_type=j...  24 us
    dot_general x16, matrix products, attend_block(): jnp.einsum('qhd,khd->hqk', query_nope, key_nope.reshape(number, att_heads...  22.4 us
    another operation x1, loops' own time, per_device(): lax.scan(one_block, carried, jnp.arange(number // size, dtype=jnp.int32))  20.8 us
    reduce_max x16, other arithmetic, update_state(): new_max = jnp.maximum(last_total + stabilizer, jnp.max(weight_log, axis=-1))  20.3 us
    while x4, local copies, waits for them, and re-layouts, per_device(): lax.scan(one_block, carried, jnp.arange(number // size, dtype=jnp.int32))  16.1 us
  transfers between devices with their start and end apart: 4, of which 2 were waited for; matrix products, arithmetic and copies ran while one was open for 17% of the time, Pallas kernels for 0%

profile of v1, /device:TPU:230, one launch (start us, length us, event | category | flops | bytes accessed | tf_op | source)
XLA Modules:
  0.0 460.4 jit_solution(2299031717601269815)
XLA Ops:
  15.7 27.1 %all-to-all-done = bf16[8,64,2048]{2,1,0:T(8,128)(2,1)S(1)} async-done(((bf16[8,64,2048]{2,1,0:T(8,128)(2,1)}), bf16[8,64,2048]{2,1,0:T(8,128)(2,1)S(1)}, u32[]{:S(2)}, u32[]{:S(2)}) %all-to-all-start) | async-done | bytes 2097184 | tf_op jit(solution)/shard_map/all_to_all | solution.py:27
  55.6 43.0 %while.47 = (s32[]{:T(128)}, f32[1,256,128]{2,1,0:T(8,128)S(1)}, f32[1,128]{1,0:T(1,128)S(1)}, f32[1]{0:T(128)}, f32[8,1,64]{2,1,0:T(1,128)S(1)}, /*index=5*/f32...) while((s32[]{:T(128)}, f32[1,256,128]{2,1,0:T(8,128)S(1)}, ...), condition=%wide.region_4.5_spmd.clone, body=%wide.region_1.0_spmd.clone.sunk | while | flops 25383812 | bytes 401378 | solution.py:282
  98.7 13.5 %all-gather.2 = f32[4,259,128]{2,1,0:T(8,128)S(1)} all-gather(f32[1,259,128]{2,1,0:T(8,128)S(1)} %maximum_bitcast_fusion), channel_id=2, replica_groups=mesh['sp_0'=8,'sp_1'=4,'tp'=8] {'sp_1'}, dimensions={0}, use_global_device_ids=true | all-gather | bytes 663040 | tf_op jit(solution)/shard_map/all_gather | solution.py:55
  125.3 13.1 %all_gather.22 = bf16[512,512]{0,1:T(8,128)(2,1)S(1)} all-gather(bf16[512,64]{0,1:T(8,128)(2,1)S(1)} %copy-done.14), channel_id=1, replica_groups=mesh['sp_0'=8,'sp_1'=4,'tp'=8] {'tp'}, dimensions={1}, use_global_device_ids=true | all-gather | bytes 589824 | tf_op jit(solution)/shard_map/all_gather | solution.py:256
  147.3 10.8 %all-to-all-done.1 = bf16[8,512,96]{1,2,0:T(8,128)(2,1)S(1)} async-done(((bf16[8,512,96]{1,2,0:T(8,128)(2,1)}), bf16[8,512,96]{1,2,0:T(8,128)(2,1)S(1)}, u32[]{:S(2)}, u32[]{:S(2)}) %all-to-all-start.1) | async-done | bytes 786464 | tf_op jit(solution)/shard_map/all_to_all | solution.py:253
  186.3 74.6 %while.45 = (s32[]{:T(128)}, f32[1,256,128]{2,1,0:T(8,128)S(1)}, f32[1,128]{1,0:T(1,128)S(1)}, f32[1]{0:T(128)}, f32[8,1,64,256]{3,2,1,0:T(8,128)S(1)}, /*index=...) while((s32[]{:T(128)}, f32[1,256,128]{2,1,0:T(8,128)S(1)}, ...), condition=%wide.region_11.12_spmd, body=%wide.region_6.11_spmd.sunk | while | flops 69588096 | bytes 982777 | solution.py:295
  261.1 13.7 %psum.7 = f32[512]{0:T(512)S(1)} all-reduce(f32[512]{0:T(512)S(1)} %reduce_sum.82), channel_id=1, replica_groups=mesh['sp_0'=8,'sp_1'=4,'tp'=8] {'tp'}, use_global_device_ids=true, to_apply=%region_13.14 | all-reduce | flops 512 | bytes 4096 | tf_op jit(solution)/shard_map/psum | solution.py:299
  277.7 6.0 %fusion.165 = (bf16[16384,128]{0,1:T(8,128)(2,1)}, bf16[16384,128]{0,1:T(8,128)(2,1)}) fusion(bf16[16384,320]{0,1:T(8,128)(2,1)} %all-gather.7.cloned.1.call-done), kind=kLoop, calls=%fused_computation.270 | loop fusion | bytes 16777216 | tf_op jit(solution)/shard_map/split | solution.py:85
  283.7 6.4 %copy.49 = bf16[16384,128]{1,0:T(8,128)(2,1)} copy(bf16[16384,128]{0,1:T(8,128)(2,1)} %get-tuple-element.494) | data formatting | bytes 8388608 | tf_op jit(solution)/shard_map/while | solution.py:376
  294.9 6.4 %copy.46 = bf16[16384,128]{1,0:T(8,128)(2,1)} copy(bf16[16384,128]{0,1:T(8,128)(2,1)} %get-tuple-element.495) | data formatting | bytes 8388608 | tf_op jit(solution)/shard_map/while | solution.py:376
  301.4 118.3 %while.46 = (s32[]{:T(128)}, f32[1,512]{1,0:T(1,128)S(1)}, f32[1,512]{1,0:T(1,128)S(1)}, f32[1,512,128]{2,1,0:T(8,128)S(1)}, s32[16]{0:T(128)S(1)}, /*index=5*/s...) while((s32[]{:T(128)}, f32[1,512]{1,0:T(1,128)S(1)}, ...), condition=%wide.region_21.22_spmd, body=%wide.region_16.21_spmd.sunk | while | flops 340396032 | bytes 12036461 | solution.py:376
  318.6 4.9 %conditional.2 = ((f32[1,512]{1,0:T(1,128)S(1)}, f32[1,512]{1,0:T(1,128)S(1)}, f32[1,512,128]{2,1,0:T(8,128)S(1)})) conditional(s32[]{:T(128)} %convert_element_type.205, (f32[1,512]{1,0:T(1,128)S(1)}, f32[1,512]{1,0:T(1,128)S(1)}, f32[1,512,128]{2,1,0:T(8,128)S(1)}) %tuple.113, (s32[]{:T(128)}, s32[512]{0:T(512)S(1)}, ...), branch_computations={%region_17.17_spmd, %region_18.20_spmd} | conditional | flops 340396032 | bytes 12036178 | solution.py:372
  326.0 4.9 %conditional.2 = ((f32[1,512]{1,0:T(1,128)S(1)}, f32[1,512]{1,0:T(1,128)S(1)}, f32[1,512,128]{2,1,0:T(8,128)S(1)})) conditional(s32[]{:T(128)} %convert_element_type.205, (f32[1,512]{1,0:T(1,128)S(1)}, f32[1,512]{1,0:T(1,128)S(1)}, f32[1,512,128]{2,1,0:T(8,128)S(1)}) %tuple.113, (s32[]{:T(128)}, s32[512]{0:T(512)S(1)}, ...), branch_computations={%region_17.17_spmd, %region_18.20_spmd} | conditional | flops 340396032 | bytes 12036178 | solution.py:372
  333.4 4.9 %conditional.2 = ((f32[1,512]{1,0:T(1,128)S(1)}, f32[1,512]{1,0:T(1,128)S(1)}, f32[1,512,128]{2,1,0:T(8,128)S(1)})) conditional(s32[]{:T(128)} %convert_element_type.205, (f32[1,512]{1,0:T(1,128)S(1)}, f32[1,512]{1,0:T(1,128)S(1)}, f32[1,512,128]{2,1,0:T(8,128)S(1)}) %tuple.113, (s32[]{:T(128)}, s32[512]{0:T(512)S(1)}, ...), branch_computations={%region_17.17_spmd, %region_18.20_spmd} | conditional | flops 340396032 | bytes 12036178 | solution.py:372
  340.8 4.9 %conditional.2 = ((f32[1,512]{1,0:T(1,128)S(1)}, f32[1,512]{1,0:T(1,128)S(1)}, f32[1,512,128]{2,1,0:T(8,128)S(1)})) conditional(s32[]{:T(128)} %convert_element_type.205, (f32[1,512]{1,0:T(1,128)S(1)}, f32[1,512]{1,0:T(1,128)S(1)}, f32[1,512,128]{2,1,0:T(8,128)S(1)}) %tuple.113, (s32[]{:T(128)}, s32[512]{0:T(512)S(1)}, ...), branch_computations={%region_17.17_spmd, %region_18.20_spmd} | conditional | flops 340396032 | bytes 12036178 | solution.py:372
  348.2 4.9 %conditional.2 = ((f32[1,512]{1,0:T(1,128)S(1)}, f32[1,512]{1,0:T(1,128)S(1)}, f32[1,512,128]{2,1,0:T(8,128)S(1)})) conditional(s32[]{:T(128)} %convert_element_type.205, (f32[1,512]{1,0:T(1,128)S(1)}, f32[1,512]{1,0:T(1,128)S(1)}, f32[1,512,128]{2,1,0:T(8,128)S(1)}) %tuple.113, (s32[]{:T(128)}, s32[512]{0:T(512)S(1)}, ...), branch_computations={%region_17.17_spmd, %region_18.20_spmd} | conditional | flops 340396032 | bytes 12036178 | solution.py:372
  355.6 4.9 %conditional.2 = ((f32[1,512]{1,0:T(1,128)S(1)}, f32[1,512]{1,0:T(1,128)S(1)}, f32[1,512,128]{2,1,0:T(8,128)S(1)})) conditional(s32[]{:T(128)} %convert_element_type.205, (f32[1,512]{1,0:T(1,128)S(1)}, f32[1,512]{1,0:T(1,128)S(1)}, f32[1,512,128]{2,1,0:T(8,128)S(1)}) %tuple.113, (s32[]{:T(128)}, s32[512]{0:T(512)S(1)}, ...), branch_computations={%region_17.17_spmd, %region_18.20_spmd} | conditional | flops 340396032 | bytes 12036178 | solution.py:372
  363.0 4.9 %conditional.2 = ((f32[1,512]{1,0:T(1,128)S(1)}, f32[1,512]{1,0:T(1,128)S(1)}, f32[1,512,128]{2,1,0:T(8,128)S(1)})) conditional(s32[]{:T(128)} %convert_element_type.205, (f32[1,512]{1,0:T(1,128)S(1)}, f32[1,512]{1,0:T(1,128)S(1)}, f32[1,512,128]{2,1,0:T(8,128)S(1)}) %tuple.113, (s32[]{:T(128)}, s32[512]{0:T(512)S(1)}, ...), branch_computations={%region_17.17_spmd, %region_18.20_spmd} | conditional | flops 340396032 | bytes 12036178 | solution.py:372
  370.4 4.9 %conditional.2 = ((f32[1,512]{1,0:T(1,128)S(1)}, f32[1,512]{1,0:T(1,128)S(1)}, f32[1,512,128]{2,1,0:T(8,128)S(1)})) conditional(s32[]{:T(128)} %convert_element_type.205, (f32[1,512]{1,0:T(1,128)S(1)}, f32[1,512]{1,0:T(1,128)S(1)}, f32[1,512,128]{2,1,0:T(8,128)S(1)}) %tuple.113, (s32[]{:T(128)}, s32[512]{0:T(512)S(1)}, ...), branch_computations={%region_17.17_spmd, %region_18.20_spmd} | conditional | flops 340396032 | bytes 12036178 | solution.py:372
  377.8 4.9 %conditional.2 = ((f32[1,512]{1,0:T(1,128)S(1)}, f32[1,512]{1,0:T(1,128)S(1)}, f32[1,512,128]{2,1,0:T(8,128)S(1)})) conditional(s32[]{:T(128)} %convert_element_type.205, (f32[1,512]{1,0:T(1,128)S(1)}, f32[1,512]{1,0:T(1,128)S(1)}, f32[1,512,128]{2,1,0:T(8,128)S(1)}) %tuple.113, (s32[]{:T(128)}, s32[512]{0:T(512)S(1)}, ...), branch_computations={%region_17.17_spmd, %region_18.20_spmd} | conditional | flops 340396032 | bytes 12036178 | solution.py:372
  385.2 4.9 %conditional.2 = ((f32[1,512]{1,0:T(1,128)S(1)}, f32[1,512]{1,0:T(1,128)S(1)}, f32[1,512,128]{2,1,0:T(8,128)S(1)})) conditional(s32[]{:T(128)} %convert_element_type.205, (f32[1,512]{1,0:T(1,128)S(1)}, f32[1,512]{1,0:T(1,128)S(1)}, f32[1,512,128]{2,1,0:T(8,128)S(1)}) %tuple.113, (s32[]{:T(128)}, s32[512]{0:T(512)S(1)}, ...), branch_computations={%region_17.17_spmd, %region_18.20_spmd} | conditional | flops 340396032 | bytes 12036178 | solution.py:372
  392.6 4.9 %conditional.2 = ((f32[1,512]{1,0:T(1,128)S(1)}, f32[1,512]{1,0:T(1,128)S(1)}, f32[1,512,128]{2,1,0:T(8,128)S(1)})) conditional(s32[]{:T(128)} %convert_element_type.205, (f32[1,512]{1,0:T(1,128)S(1)}, f32[1,512]{1,0:T(1,128)S(1)}, f32[1,512,128]{2,1,0:T(8,128)S(1)}) %tuple.113, (s32[]{:T(128)}, s32[512]{0:T(512)S(1)}, ...), branch_computations={%region_17.17_spmd, %region_18.20_spmd} | conditional | flops 340396032 | bytes 12036178 | solution.py:372
  407.4 4.9 %conditional.2 = ((f32[1,512]{1,0:T(1,128)S(1)}, f32[1,512]{1,0:T(1,128)S(1)}, f32[1,512,128]{2,1,0:T(8,128)S(1)})) conditional(s32[]{:T(128)} %convert_element_type.205, (f32[1,512]{1,0:T(1,128)S(1)}, f32[1,512]{1,0:T(1,128)S(1)}, f32[1,512,128]{2,1,0:T(8,128)S(1)}) %tuple.113, (s32[]{:T(128)}, s32[512]{0:T(512)S(1)}, ...), branch_computations={%region_17.17_spmd, %region_18.20_spmd} | conditional | flops 340396032 | bytes 12036178 | solution.py:372
  422.6 29.8 %all_to_all.15 = bf16[8,64,2048]{2,1,0:T(8,128)(2,1)S(1)} all-to-all(bf16[8,64,2048]{2,1,0:T(8,128)(2,1)S(1)} %bitcast.456), channel_id=1, replica_groups=mesh['sp_0'=8,'sp_1'=4,'tp'=8] {'tp'}, dimensions={0} | all-to-all | bytes 4194304 | tf_op jit(solution)/shard_map/all_to_all | solution.py:96
  (459 shorter events, 262.9 us)
Async XLA Ops:
  6.5 268.4 %copy-start = (bf16[256,2048]{1,0:T(8,128)(2,1)S(1)}, bf16[256,2048]{1,0:T(8,128)(2,1)}, u32[]{:S(2)}) copy-start(bf16[256,2048]{1,0:T(8,128)(2,1)} %param.46) | copy-start | bytes 3145732
  11.1 31.6 %all-to-all-start = ((bf16[8,64,2048]{2,1,0:T(8,128)(2,1)}), bf16[8,64,2048]{2,1,0:T(8,128)(2,1)S(1)}, u32[]{:S(2)}, u32[]{:S(2)}) async-start(bf16[8,64,2048]{2,1,0:T(8,128)(2,1)} %broadcast_in_dim.36), calls=%async_computation | async-start | bytes 4194304 | tf_op jit(solution)/shard_map/all_to_all | solution.py:27
  15.6 28.7 %copy-start.21 = (f32[512,1]{0,1:T(1,128)S(1)}, f32[512,1]{0,1:T(1,128)}, u32[]{:S(2)}) copy-start(f32[512,1]{0,1:T(1,128)} %param.36) | copy-start | bytes 6148
  15.6 144.9 %all-gather.9.cloned.1.call-start = ((), (), s32[]{:S(2)}) async-start(), calls=%async_computation.4 | async-start | bytes 1216512 | tf_op jit(solution)/shard_map/all_gather | solution.py:55
  42.7 4.3 copy-start.11
  48.5 2.8 copy-start.4
  55.6 69.7 %copy-start.15 = (bf16[512,64]{0,1:T(8,128)(2,1)S(1)}, bf16[512,64]{0,1:T(8,128)(2,1)}, u32[]{:S(2)}) copy-start(bf16[512,64]{0,1:T(8,128)(2,1)} %convolution_convert_fusion.8) | copy-start | bytes 196612
  55.6 69.7 %copy-start.14 = (bf16[512,64]{0,1:T(8,128)(2,1)S(1)}, bf16[512,64]{0,1:T(8,128)(2,1)}, u32[]{:S(2)}) copy-start(bf16[512,64]{0,1:T(8,128)(2,1)} %convolution_convert_fusion.9) | copy-start | bytes 196612
  98.6 24.0 %copy-start.17 = (f32[8,1,64]{2,1,0:T(1,128)}, f32[8,1,64]{2,1,0:T(1,128)S(1)}, u32[]{:S(2)}) copy-start(f32[8,1,64]{2,1,0:T(1,128)S(1)} %get-tuple-element.858) | copy-start | bytes 6148
  98.7 40.3 %copy-start.24 = (bf16[512,128]{1,0:T(8,128)(2,1)S(1)}, bf16[512,128]{1,0:T(8,128)(2,1)}, u32[]{:S(2)}) copy-start(bf16[512,128]{1,0:T(8,128)(2,1)} %param.45) | copy-start | bytes 393220
  98.7 40.3 %copy-start.26 = (f32[512]{0:T(512)S(1)}, f32[512]{0:T(512)}, u32[]{:S(2)}) copy-start(f32[512]{0:T(512)} %param.42) | copy-start | bytes 6148
  112.2 27.1 %copy-start.25 = (bf16[512,128]{1,0:T(8,128)(2,1)S(1)}, bf16[512,128]{1,0:T(8,128)(2,1)}, u32[]{:S(2)}) copy-start(bf16[512,128]{1,0:T(8,128)(2,1)} %param.44) | copy-start | bytes 393220
  125.2 152.6 %all-gather.7.cloned.1.call-start = ((), (), s32[]{:S(2)}) async-start(), calls=%async_computation.3 | async-start | bytes 10813440 | tf_op jit(solution)/shard_map/all_gather | solution.py:85
  125.2 13.7 %copy-start.18 = (f32[32]{0:T(128)}, f32[32]{0:T(128)S(1)}, u32[]{:S(2)}) copy-start(f32[32]{0:T(128)S(1)} %multiply_power_fusion) | copy-start | bytes 388
  139.3 7.1 %copy-start.7 = (bf16[512,128]{1,0:T(8,128)(2,1)S(1)}, bf16[512,128]{1,0:T(8,128)(2,1)}, u32[]{:S(2)}) copy-start(bf16[512,128]{1,0:T(8,128)(2,1)} %convolution_convert_fusion.6) | copy-start | bytes 393220
  140.4 17.8 %copy-start.16 = (f32[768]{0:T(1024)S(1)}, f32[768]{0:T(1024)}, u32[]{:S(2)}) copy-start(f32[768]{0:T(1024)} %param.41) | copy-start | bytes 9220
  141.4 16.6 %all-to-all-start.1 = ((bf16[8,512,96]{1,2,0:T(8,128)(2,1)}), bf16[8,512,96]{1,2,0:T(8,128)(2,1)S(1)}, u32[]{:S(2)}, u32[]{:S(2)}) async-start(bf16[8,512,96]{1,2,0:T(8,128)(2,1)} %stack.2), calls=%async_computation.1 | async-start | bytes 1572864 | tf_op jit(solution)/shard_map/all_to_all | solution.py:253
  147.3 12.2 %copy-start.19 = (f32[32]{0:T(128)S(1)}, f32[32]{0:T(128)}, u32[]{:S(2)}) copy-start(f32[32]{0:T(128)} %copy-done.18) | copy-start | bytes 388
  158.3 25.6 %copy-start.20 = (f32[1,1,128]{2,1,0:T(1,128)S(1)}, f32[1,1,128]{2,1,0:T(1,128)}, u32[]{:S(2)}) copy-start(f32[1,1,128]{2,1,0:T(1,128)} %get-tuple-element.488) | copy-start | bytes 1540
  159.0 27.2 %copy-start.3 = (f32[8,1,64,256]{3,2,1,0:T(8,128)S(1)}, f32[8,1,64,256]{3,2,1,0:T(8,128)}, u32[]{:S(2)}) copy-start(f32[8,1,64,256]{3,2,1,0:T(8,128)} %custom-call.2) | copy-start | bytes 1572868
  186.3 88.5 %copy-start.13 = (bf16[512,256]{1,0:T(8,128)(2,1)S(1)}, bf16[512,256]{1,0:T(8,128)(2,1)}, u32[]{:S(2)}) copy-start(bf16[512,256]{1,0:T(8,128)(2,1)} %convolution_convert_fusion) | copy-start | bytes 786436
  294.9 6.4 %copy-start.2 = (bf16[512,1,64]{0,2,1:T(8,128)(2,1)S(1)}, bf16[512,1,64]{0,2,1:T(8,128)(2,1)}, u32[]{:S(2)}) copy-start(bf16[512,1,64]{0,2,1:T(8,128)(2,1)} %pad_maximum_fusion.1) | copy-start | bytes 196612
  301.3 118.3 %copy-start.6 = (bf16[128,2048]{1,0:T(8,128)(2,1)S(1)}, bf16[128,2048]{1,0:T(8,128)(2,1)}, u32[]{:S(2)}) copy-start(bf16[128,2048]{1,0:T(8,128)(2,1)} %param.47) | copy-start | bytes 1572868
  422.6 30.9 %copy-start.1 = (bf16[256,2048]{1,0:T(8,128)(2,1)S(1)}, bf16[256,2048]{1,0:T(8,128)(2,1)}, u32[]{:S(2)}) copy-start(bf16[256,2048]{1,0:T(8,128)(2,1)} %param.46) | copy-start | bytes 3145732
  (8 other events, 14.4 us)
Sparse Core Ops, SparseCore 0:
  125.3 34.7 all-gather.8
  162.6 110.8 all-gather.6
